TPU v7x, 32 devices: a whole 2x2x4 slice. The times are simulated.
32 devices in a mesh: rep: 4 (over z), fs: 4 (over y, x), tp: 2 (over core).
Axes of the slice: x: 2, y: 2, z: 4, core: 2. Of those that a mesh axis runs over, the one named last changes fastest.
Arguments:
- inputs: bfloat16 [4096, 2048], P(('rep', 'fs', 'tp')), may hold values from -6 to 6
- out_grad: bfloat16 [4096, 2048], P(('rep', 'fs', 'tp')), may hold values from -6 to 6
- pre_act: bfloat16 [4096, 8192], P('rep', ('fs', 'tp')), may hold values from -6 to 6
- w_up: bfloat16 [2048, 8192], P('rep', ('fs', 'tp')), may hold values from -0.125 to 0.125
- w_down_t: bfloat16 [2048, 8192], P('rep', ('fs', 'tp')), may hold values from -0.0625 to 0.0625
Outputs:
- grad_in: bfloat16 [4096, 2048], P(('rep', 'fs', 'tp'))
- grad_up: float32 [2048, 8192], P('rep', ('fs', 'tp'))
- grad_down_t: float32 [2048, 8192], P('rep', ('fs', 'tp'))
All inputs are finite; a program needn't handle non-finite values.
Results may differ from a plain program's by a relative error of at most 0.014.
Values may be sent and summed in bfloat16 or wider, within the bound.
A program may use at most 128 MiB of HBM per device.

v0:
```python
import jax
import jax.numpy as jnp
from jax import lax
from jax.sharding import PartitionSpec as P


def on_device(inputs, out_grad, pre_act, w_up, w_down_t):
    input_rows, grad_rows = (
        lax.all_gather(inputs, ("fs", "tp"), axis=0, tiled=True),
        lax.all_gather(out_grad, ("fs", "tp"), axis=0, tiled=True),
    )
    row_count, col_count = pre_act.shape
    pre_float = pre_act.astype(jnp.float32)
    linear = jnp.maximum(pre_float, 0.0)
    squared = (linear * linear).astype(jnp.bfloat16)
    grad_squared = jnp.dot(
        grad_rows,
        lax.all_gather(w_down_t, "rep", axis=0, tiled=True),
        preferred_element_type=jnp.float32,
    )
    grad_pre = (grad_squared * 2.0 * linear).astype(jnp.bfloat16)
    partial_terms = lax.dot_general(
        grad_pre,
        lax.all_gather(w_up, "rep", axis=0, tiled=True),
        (((1,), (1,)), ((), ())),
        preferred_element_type=jnp.float32,
    ).astype(jnp.bfloat16)
    grad_in = lax.psum_scatter(
        partial_terms.astype(jnp.float32).astype(jnp.bfloat16),
        ("fs", "tp"),
        scatter_dimension=0,
        tiled=True,
    )
    total_tokens = row_count * lax.axis_size("rep")
    factor = float(total_tokens) ** (-0.5)
    down_part = lax.dot_general(
        grad_rows, squared, (((0,), (0,)), ((), ())), preferred_element_type=jnp.float32
    )
    up_part = lax.dot_general(
        input_rows, grad_pre, (((0,), (0,)), ((), ())), preferred_element_type=jnp.float32
    )
    stacked = lax.psum_scatter(
        (jnp.concatenate([down_part, up_part], axis=1) * factor).astype(jnp.bfloat16),
        "rep",
        scatter_dimension=0,
        tiled=True,
    ).astype(jnp.float32)
    grad_down_t = stacked[:, :col_count]
    grad_up = stacked[:, col_count:]
    return (grad_in, grad_up, grad_down_t)


def solution(mesh):
    in_specs = (
        P(("rep", "fs", "tp"), None),
        P(("rep", "fs", "tp"), None),
        P("rep", ("fs", "tp")),
        P("rep", ("fs", "tp")),
        P("rep", ("fs", "tp")),
    )
    out_specs = (P(("rep", "fs", "tp"), None), P("rep", ("fs", "tp")), P("rep", ("fs", "tp")))
    return jax.shard_map(
        on_device, mesh=mesh, in_specs=in_specs, out_specs=out_specs, check_vma=False
    )
```

profile of v0, /device:TPU:0, one launch (start us, length us, event | category | flops | bytes accessed | tf_op | source)
XLA Modules:
  0.0 458.5 jit_solution(11764382786972358349)
XLA Ops:
  7.2 0.0 all-gather.5.cloned.1.call-start
  7.2 0.7 all-gather.5.cloned.1.call-update
  7.9 0.0 all-gather.7.cloned.1.call-start
  7.9 0.7 all-gather.7.cloned.1.call-update
  8.6 0.0 all-gather.11.cloned.1.call-start
  8.7 0.7 all-gather.11.cloned.1.call-update
  9.4 0.0 all-gather.9.cloned.1.call-start
  9.4 0.5 all-gather.9.cloned.1.call-update
  10.0 0.0 reduce-scatter.5.cloned.1.call-start
  10.0 39.2 %all-gather.5.cloned.1.call-done = bf16[1024,2048]{1,0:T(8,128)(2,1)} async-done(((bf16[128,2048]{1,0:T(8,128)(2,1)}), bf16[1024,2048]{1,0:T(8,128)(2,1)}) %all-gather.5.cloned.1.call-update) | async-done | bytes 4194320 | tf_op jit(solution)/shard_map/all_gather | solution.py:10
  49.2 11.0 %convolution_bitcast_fusion.1 = f32[2048,1024]{0,1:T(8,128)} fusion(bf16[1024,2048]{1,0:T(8,128)(2,1)} %all-gather.5.cloned.1.call-done, bf16[1024,1024]{1,0:T(8,128)(2,1)} %param.7), kind=kOutput, calls=%fused_computation.3 | convolution fusion | flops 4299161600 | bytes 14680064 | tf_op jit(solution)/shard_map/dot_general | solution.py:36
  60.2 71.4 %all-gather.7.cloned.1.call-done = bf16[2048,1024]{1,0:T(8,128)(2,1)} async-done(((bf16[512,1024]{1,0:T(8,128)(2,1)}), bf16[2048,1024]{1,0:T(8,128)(2,1)}) %all-gather.7.cloned.1.call-update) | async-done | bytes 4194320 | tf_op jit(solution)/shard_map/all_gather | solution.py:18
  131.5 9.3 %multiply_convert_fusion.1 = bf16[1024,1024]{1,0:T(8,128)(2,1)} fusion(bf16[1024,1024]{1,0:T(8,128)(2,1)S(1)} %copy-done.1, bf16[1024,2048]{1,0:T(8,128)(2,1)} %all-gather.5.cloned.1.call-done, bf16[2048,1024]{1,0:T(8,128)(2,1)} %all-gather.7.cloned.1.call-done), kind=kOutput, calls=%fused_computation.5 | convolution fusion | flops 4300210176 | bytes 12582912 | tf_op jit(solution)/shard_map/dot_general | solution.py:16
  140.8 27.7 %all-gather.11.cloned.1.call-done = bf16[1024,2048]{1,0:T(8,128)(2,1)} async-done(((bf16[128,2048]{1,0:T(8,128)(2,1)}), bf16[1024,2048]{1,0:T(8,128)(2,1)}) %all-gather.11.cloned.1.call-update) | async-done | bytes 4194320 | tf_op jit(solution)/shard_map/all_gather | solution.py:9
  168.5 7.3 %convolution_bitcast_fusion = f32[2048,1024]{0,1:T(8,128)S(1)} fusion(bf16[1024,1024]{1,0:T(8,128)(2,1)} %multiply_convert_fusion.1, bf16[1024,2048]{1,0:T(8,128)(2,1)} %all-gather.11.cloned.1.call-done), kind=kOutput, calls=%fused_computation.2 | convolution fusion | flops 4294967296 | bytes 14680064 | tf_op jit(solution)/shard_map/dot_general | solution.py:39
  175.8 4.8 %fusion = bf16[2048,2048]{0,1:T(8,128)(2,1)} fusion(f32[2048,1024]{0,1:T(8,128)S(1)} %convolution_bitcast_fusion, f32[2048,1024]{0,1:T(8,128)S(1)} %copy-done), kind=kLoop, calls=%fused_computation.1 | loop fusion | flops 12582912 | bytes 25165824 | tf_op jit(solution)/shard_map/convert_element_type | solution.py:43
  180.7 0.2 reduce-scatter.3.cloned.1.call-start
  180.9 69.8 %all-gather.9.cloned.1.call-done = bf16[2048,1024]{1,0:T(8,128)(2,1)} async-done(((bf16[512,1024]{1,0:T(8,128)(2,1)}), bf16[2048,1024]{1,0:T(8,128)(2,1)}) %all-gather.9.cloned.1.call-update) | async-done | bytes 4194320 | tf_op jit(solution)/shard_map/all_gather | solution.py:24
  250.7 8.2 %convolution_convert_fusion = bf16[1024,2048]{1,0:T(8,128)(2,1)} fusion(bf16[1024,1024]{1,0:T(8,128)(2,1)S(1)} %copy-done.2, bf16[2048,1024]{1,0:T(8,128)(2,1)} %all-gather.9.cloned.1.call-done), kind=kOutput, calls=%fused_computation.7 | convolution fusion | flops 4297064448 | bytes 10485760 | tf_op jit(solution)/shard_map/dot_general | solution.py:22
  259.0 137.1 %reduce-scatter.5.cloned.1.call-done = bf16[512,2048]{0,1:T(8,128)(2,1)} async-done(((bf16[2048,2048]{0,1:T(8,128)(2,1)}), bf16[512,2048]{0,1:T(8,128)(2,1)}) %reduce-scatter.5.cloned.1.call-update) | async-done | bytes 2097168 | tf_op jit(solution)/shard_map/reduce_scatter | solution.py:42
  396.1 3.5 fusion.3
  399.5 2.9 copy.9
  402.4 1.8 copy.8
  404.2 47.5 %reduce-scatter.3.cloned.1.call-done = bf16[128,2048]{1,0:T(8,128)(2,1)} async-done(((bf16[1024,2048]{1,0:T(8,128)(2,1)}), bf16[128,2048]{1,0:T(8,128)(2,1)}) %reduce-scatter.3.cloned.1.call-update) | async-done | bytes 524304 | tf_op jit(solution)/shard_map/reduce_scatter | solution.py:28
  (8 shorter events, 0.0 us)
Async XLA Ops:
  7.2 42.0 %all-gather.5.cloned.1.call-start = ((), (), s32[]{:S(2)}) async-start(), calls=%async_computation.2 | async-start | bytes 4718592 | tf_op jit(solution)/shard_map/all_gather | solution.py:10
  7.9 123.6 %all-gather.7.cloned.1.call-start = ((), (), s32[]{:S(2)}) async-start(), calls=%async_computation.3 | async-start | bytes 5242880 | tf_op jit(solution)/shard_map/all_gather | solution.py:18
  8.6 159.9 %all-gather.11.cloned.1.call-start = ((), (), s32[]{:S(2)}) async-start(), calls=%async_computation.6 | async-start | bytes 4718592 | tf_op jit(solution)/shard_map/all_gather | solution.py:9
  9.4 241.4 %all-gather.9.cloned.1.call-start = ((), (), s32[]{:S(2)}) async-start(), calls=%async_computation.4 | async-start | bytes 5242880 | tf_op jit(solution)/shard_map/all_gather | solution.py:24
  10.0 121.6 %copy-start.1 = (bf16[1024,1024]{1,0:T(8,128)(2,1)S(1)}, bf16[1024,1024]{1,0:T(8,128)(2,1)}, u32[]{:S(2)}) copy-start(bf16[1024,1024]{1,0:T(8,128)(2,1)} %param.7) | copy-start | bytes 6291460
  10.0 386.1 %reduce-scatter.5.cloned.1.call-start = ((), (), s32[]{:S(2)}) async-start(), calls=%async_computation.7 | async-start | bytes 10485760 | tf_op jit(solution)/shard_map/reduce_scatter | solution.py:42
  168.5 7.3 %copy-start = (f32[2048,1024]{0,1:T(8,128)S(1)}, f32[2048,1024]{0,1:T(8,128)}, u32[]{:S(2)}) copy-start(f32[2048,1024]{0,1:T(8,128)} %convolution_bitcast_fusion.1) | copy-start | bytes 25165828
  180.6 70.1 %copy-start.2 = (bf16[1024,1024]{1,0:T(8,128)(2,1)S(1)}, bf16[1024,1024]{1,0:T(8,128)(2,1)}, u32[]{:S(2)}) copy-start(bf16[1024,1024]{1,0:T(8,128)(2,1)} %multiply_convert_fusion.1) | copy-start | bytes 6291460
  180.7 271.0 %reduce-scatter.3.cloned.1.call-start = ((), (), s32[]{:S(2)}) async-start(), calls=%async_computation.5 | async-start | bytes 4718592 | tf_op jit(solution)/shard_map/reduce_scatter | solution.py:28
Sparse Core Ops, SparseCore 0:
  9.9 39.2 all-gather.4
  50.8 80.7 all-gather.6
  133.4 35.0 all-gather.10
  170.0 80.7 all-gather.8
  252.9 143.0 reduce-scatter.4
  399.9 51.7 reduce-scatter.2
where the time goes:
time: 459 us
  waiting for transfers between devices  395 us (86%)
  matrix products  35.8 us (8%)
  between operations  14.1 us (3%)
  local copies, waits for them, and re-layouts  8.15 us (2%)
  other arithmetic  4.82 us (1%)
    reduce_scatter x1, waiting for transfers between devices, on_device(): lax.psum_scatter((jnp.concatenate([down_part, up_part], axis=1) * factor)...  137 us
    all_gather x1, waiting for transfers between devices, on_device(): lax.all_gather(w_down_t, 'rep', axis=0, tiled=True)  71.4 us
    all_gather x1, waiting for transfers between devices, on_device(): lax.all_gather(w_up, 'rep', axis=0, tiled=True)  69.8 us
    reduce_scatter x1, waiting for transfers between devices, on_device(): lax.psum_scatter(partial_terms.astype(jnp.float32).astype(jnp.bfloat16),...  47.5 us
    all_gather x1, waiting for transfers between devices, on_device(): lax.all_gather(out_grad, ('fs', 'tp'), axis=0, tiled=True)  39.2 us
    all_gather x1, waiting for transfers between devices, on_device(): lax.all_gather(inputs, ('fs', 'tp'), axis=0, tiled=True)  27.7 us
    dot_general x1, matrix products, on_device(): lax.dot_general(grad_rows, squared, (((0,), (0,)), ((), ())), preferred_e...  11 us
    dot_general x1, matrix products, on_device(): jnp.dot(grad_rows, lax.all_gather(w_down_t, 'rep', axis=0, tiled=True), p...  9.28 us
  transfers between devices with their start and end apart: 6, of which 6 were waited for; matrix products, arithmetic and copies ran while one was open for 11% of the time, Pallas kernels for 0%

commit v1 on v0

v1 whole, which is shorter than its diff:
```python
import functools

import jax
import jax.numpy as jnp
from jax import lax
from jax.experimental import pallas as pl
from jax.experimental.pallas import tpu as pltpu
from jax.sharding import PartitionSpec as P

BF16 = jnp.bfloat16
F32 = jnp.float32


def kernel(
    n, n_fs, chunks, factor,
    x_ref, og_ref, pre_ref, wu_ref, wd_ref,
    gin_ref, gu_ref, gd_ref,
    x_all, og_all, wu_all, wd_all, sq, gp, rs, tbuf, prec, frec,
    zs, zr, xs, xr, cs, cr, ts, tr, fsend, frecv,
):
    r, f, t = lax.axis_index("rep"), lax.axis_index("fs"), lax.axis_index("tp")
    tok, d_model = og_ref.shape
    shard, cols = wd_ref.shape
    crow = shard // chunks
    partner = {"tp": 1 - t}
    peers = [None] + [{"fs": lax.rem(f + d, n_fs)} for d in range(1, n_fs)]
    ahead = ({"rep": lax.rem(r + 1, n)}, {"rep": lax.rem(r + n - 1, n)})
    depth = (r, n - 1 - r)
    has_prev = (r > 0, r < n - 1)
    has_next = (r < n - 1, r > 0)

    barrier = pltpu.get_barrier_semaphore()
    for way in range(2):
        @pl.when(has_next[way])
        def _(way=way):
            pl.semaphore_signal(barrier, inc=1, device_id=ahead[way])
    for d in range(1, n_fs):
        pl.semaphore_signal(barrier, inc=1, device_id=peers[d])
    pl.semaphore_signal(barrier, inc=1, device_id=partner)
    pl.semaphore_wait(
        barrier, n_fs + jnp.where(r > 0, 1, 0) + jnp.where(r < n - 1, 1, 0)
    )

    def remote(src, dst, send, recv, target):
        return pltpu.make_async_remote_copy(
            src_ref=src, dst_ref=dst, send_sem=send, recv_sem=recv,
            device_id=target, device_id_type=pl.DeviceIdType.MESH,
        )

    def rows_of(ref, ff, tt):
        return ref.at[pl.ds(pl.multiple_of((ff * 2 + tt) * tok, tok), tok), :]

    def z_copy(phase, way, k, j, src, dst):
        return remote(
            src, dst, zs.at[phase, way, k, j], zr.at[phase, way, k, j], ahead[way]
        )

    def piece(ref, j):
        return ref.at[pl.ds(pl.multiple_of(j * crow, crow), crow), :]

    def send_own(phase, own, everyone):
        for way in range(2):
            @pl.when(has_next[way])
            def _(way=way):
                for j in range(chunks):
                    z_copy(
                        phase, way, 0, j, piece(own, j), piece(everyone.at[r], j)
                    ).start()

    def spread_start(q, own, everyone):
        for d in range(1, n_fs):
            remote(
                own, rows_of(everyone, f, t), xs.at[q, d], xr.at[q, d], peers[d]
            ).start()
        remote(
            own, rows_of(everyone, f, t), cs.at[q, 0], cr.at[q, 0], partner
        ).start()
        everyone[pl.ds(pl.multiple_of((f * 2 + t) * tok, tok), tok), :] = own[...]

    def spread_pass(q, everyone):
        for d in range(1, n_fs):
            src = rows_of(everyone, lax.rem(f + n_fs - d, n_fs), t)
            remote(src, src, xs.at[q, d], xr.at[q, d], peers[d]).wait()
            remote(src, src, cs.at[q, d], cr.at[q, d], partner).start()

    def spread_end(q, everyone):
        for d in range(n_fs):
            there = rows_of(everyone, lax.rem(f + n_fs - d, n_fs), 1 - t)
            remote(there, there, cs.at[q, d], cr.at[q, d], partner).wait()

    spread_start(0, og_ref, og_all)
    send_own(0, wd_ref, wd_all)
    wd_all[r] = wd_ref[...]
    wu_all[r] = wu_ref[...]
    tile = 2 * tok

    def square(i, _):
        at = pl.ds(pl.multiple_of(i * tile, tile), tile)
        linear = jnp.maximum(pre_ref[at, :].astype(F32), 0.0)
        sq[at, :] = (linear * linear).astype(BF16)
        return 0

    lax.fori_loop(0, n_fs, square, 0)
    spread_pass(0, og_all)
    spread_end(0, og_all)
    spread_start(1, x_ref, x_all)

    def partial(left, right, s, j):
        at = pl.ds(pl.multiple_of(s * shard + j * crow, crow), crow)
        return lax.dot_general(
            left[:, at], right[...], (((0,), (0,)), ((), ())),
            preferred_element_type=F32,
        ) * factor

    def one_round(phase, everyone, left, right, k):
        def one_piece(j, _):
            at = pl.ds(pl.multiple_of(j * crow, crow), crow)
            for way in range(2):
                sign = 1 - 2 * way
                slots = rs.at[phase, way]

                @pl.when(k < depth[way])
                def _(way=way, sign=sign):
                    block = piece(everyone.at[r - sign * (1 + k)], j)
                    z_copy(phase, way, k, j, block, block).wait_recv()

                    @pl.when(has_next[way])
                    def _():
                        z_copy(phase, way, k + 1, j, block, block).start()

                @pl.when(k >= depth[way])
                def _(way=way, slots=slots):
                    back = k - depth[way]
                    s = n - 1 - back if way == 0 else back
                    term = partial(left, right, s, j)
                    block = piece(slots.at[s], j)

                    @pl.when(has_prev[way])
                    def _():
                        z_copy(phase, way, k, j, block, block).wait_recv()
                        slots[s, at, :] = (term + slots[s, at, :].astype(F32)).astype(BF16)

                    @pl.when(jnp.logical_not(has_prev[way]))
                    def _():
                        slots[s, at, :] = term.astype(BF16)

                    z_copy(phase, way, k + 1, j, block, block).start()
            return 0

        lax.fori_loop(0, chunks, one_piece, 0)

    def last_round(phase, left, right, out):
        def one_piece(j, _):
            at = pl.ds(pl.multiple_of(j * crow, crow), crow)
            out[at, :] = partial(left, right, r, j)
            for way in range(2):
                @pl.when(has_prev[way])
                def _(way=way):
                    block = piece(rs.at[phase, way, r], j)
                    z_copy(phase, way, n - 1, j, block, block).wait_recv()
                    out[at, :] += rs[phase, way, r, at, :].astype(F32)
            return 0

        lax.fori_loop(0, chunks, one_piece, 0)

    def round_down(k, _):
        one_round(0, wd_all, og_all, sq, k)
        return 0

    lax.fori_loop(0, n - 1, round_down, 0)
    send_own(1, wu_ref, wu_all)
    spread_pass(1, x_all)

    def make_grad_pre(i, _):
        at = pl.ds(pl.multiple_of(i * tile, tile), tile)
        total = jnp.zeros((tile, cols), F32)
        for s in range(n):
            total += jnp.dot(
                og_all[at, s * shard:(s + 1) * shard], wd_all[s],
                preferred_element_type=F32,
            )
        linear = jnp.maximum(pre_ref[at, :].astype(F32), 0.0)
        gp[at, :] = (total * 2.0 * linear).astype(BF16)
        return 0

    lax.fori_loop(0, n_fs, make_grad_pre, 0)
    spread_end(1, x_all)
    last_round(0, og_all, sq, gd_ref)

    def cross(s):
        return remote(tbuf.at[s, 1 - t], prec.at[s], ts.at[s], tr.at[s], partner)

    def out_copy(s, d):
        rows = pl.ds(pl.multiple_of(lax.rem(f + d, n_fs) * tok, tok), tok)
        return remote(
            prec.at[s, rows, :], frec.at[s, d - 1],
            fsend.at[s, d], frecv.at[s, d], peers[d],
        )

    def block_term(s):
        def body(i, _):
            at = pl.ds(pl.multiple_of(i * tile, tile), tile)
            here = pl.ds(pl.multiple_of(i * tok, tok), tok)
            term = lax.dot_general(
                gp[at, :], wu_all[s], (((1,), (1,)), ((), ())),
                preferred_element_type=F32,
            ).astype(BF16)
            tbuf[s, 0, here, :] = term[:tok]
            tbuf[s, 1, here, :] = term[tok:]
            return 0

        lax.fori_loop(0, n_fs, body, 0)
        cross(s).start()

    def chip_sum(s):
        cross(s).wait()

        def body(i, _):
            here = pl.ds(pl.multiple_of(i * tok, tok), tok)
            prec[s, here, :] = (
                prec[s, here, :].astype(F32) + tbuf[s, t, here, :].astype(F32)
            ).astype(BF16)
            return 0

        lax.fori_loop(0, n_fs, body, 0)
        for d in range(1, n_fs):
            out_copy(s, d).start()

    def for_new(k, work):
        def body(way, _):
            @pl.when(jnp.where(way == 0, k < r, k < n - 1 - r))
            def _():
                work(jnp.where(way == 0, r - 1 - k, r + 1 + k))
            return 0

        lax.fori_loop(0, 2, body, 0)

    block_term(r)

    def round_up(k, _):
        one_round(1, wu_all, x_all, gp, k)
        for_new(k, block_term)

        @pl.when(k == 0)
        def _():
            chip_sum(r)

        @pl.when(k > 0)
        def _():
            for_new(k - 1, chip_sum)
        return 0

    lax.fori_loop(0, n - 1, round_up, 0)
    for_new(n - 2, chip_sum)
    last_round(1, x_all, gp, gu_ref)

    own_rows = pl.ds(pl.multiple_of(f * tok, tok), tok)
    for s in range(n):
        total = prec[s, own_rows, :].astype(F32)
        for d in range(1, n_fs):
            out_copy(s, d).wait()
            total += frec[s, d - 1].astype(F32)
        gin_ref[:, s * shard:(s + 1) * shard] = total.astype(BF16)

    for way in range(2):
        @pl.when(has_next[way])
        def _(way=way):
            def body(k, _):
                for phase in range(2):
                    for j in range(chunks):
                        block = piece(rs.at[0, 0, 0], j)
                        z_copy(phase, way, k, j, block, block).wait_send()
                return 0

            lax.fori_loop(0, n, body, 0)


def on_device(n, n_fs, inputs, out_grad, pre_act, w_up, w_down_t):
    tok, d_model = inputs.shape
    group, cols = pre_act.shape
    shard = w_up.shape[0]
    chunks = max(1, shard // 128)
    factor = float(group * n) ** -0.5
    dma = pltpu.SemaphoreType.DMA
    vmem = pl.BlockSpec(memory_space=pltpu.VMEM)
    grad_in, grad_up, grad_down_t = pl.pallas_call(
        functools.partial(kernel, n, n_fs, chunks, factor),
        out_shape=(
            jax.ShapeDtypeStruct((tok, d_model), BF16),
            jax.ShapeDtypeStruct((shard, cols), F32),
            jax.ShapeDtypeStruct((shard, cols), F32),
        ),
        in_specs=[vmem] * 5,
        out_specs=(vmem,) * 3,
        scratch_shapes=[
            pltpu.VMEM((group, d_model), BF16),
            pltpu.VMEM((group, d_model), BF16),
            pltpu.VMEM((n, shard, cols), BF16),
            pltpu.VMEM((n, shard, cols), BF16),
            pltpu.VMEM((group, cols), BF16),
            pltpu.VMEM((group, cols), BF16),
            pltpu.VMEM((2, 2, n, shard, cols), BF16),
            pltpu.VMEM((n, 2, n_fs * tok, shard), BF16),
            pltpu.VMEM((n, n_fs * tok, shard), BF16),
            pltpu.VMEM((n, n_fs - 1, tok, shard), BF16),
            dma((2, 2, n, chunks)),
            dma((2, 2, n, chunks)),
            dma((2, n_fs)),
            dma((2, n_fs)),
            dma((2, n_fs)),
            dma((2, n_fs)),
            dma((n,)),
            dma((n,)),
            dma((n, n_fs)),
            dma((n, n_fs)),
        ],
        compiler_params=pltpu.CompilerParams(
            collective_id=0, has_side_effects=True, vmem_limit_bytes=67043328
        ),
    )(inputs, out_grad, pre_act, w_up, w_down_t)
    return grad_in, grad_up, grad_down_t


def solution(mesh):
    rows = P(("rep", "fs", "tp"), None)
    blocks = P("rep", ("fs", "tp"))
    return jax.shard_map(
        functools.partial(on_device, mesh.shape["rep"], mesh.shape["fs"]),
        mesh=mesh,
        in_specs=(rows, rows, blocks, blocks, blocks),
        out_specs=(rows, blocks, blocks),
        check_vma=False,
    )
```

time: 459 us -> 204 us (0.44)
  waiting for transfers between devices: 395 us -> 0 us
  Pallas kernels: 0 us -> 197 us
  matrix products: 35.8 us -> 0 us
  between operations: 14.1 us -> 0.64 us
  other arithmetic: 4.82 us -> 0 us
    all_gather x4 -> x0, waiting for transfers between devices: 208 us -> none  [the longest x1 71.4 us: on_device(): lax.all_gather(w_down_t, 'rep', axis=0, tiled=True)]
    pallas_call x0 -> x1, Pallas kernels: none -> 197 us  [on_device(): pl.pallas_call(functools.partial(kernel, n, n_fs, chunks, factor), out_sh...]
    reduce_scatter x2 -> x0, waiting for transfers between devices: 185 us -> none  [the longest x1 137 us: on_device(): lax.psum_scatter((jnp.concatenate([down_part, up_part], axis=1) * factor)...]
    dot_general x4 -> x0, matrix products: 35.8 us -> none  [the longest x1 11 us: on_device(): lax.dot_general(grad_rows, squared, (((0,), (0,)), ((), ())), preferred_e...]
    convert_element_type x1 -> x0, other arithmetic: 4.82 us -> none  [on_device(): (jnp.concatenate([down_part, up_part], axis=1) * factor).astype(jnp.bfloa...]
  transfers between devices with their start and end apart: 6 -> 0, of which waited for: 6 -> 0; matrix products, arithmetic and copies ran while one was open for 11% -> 0% of each run, Pallas kernels for 0% -> 0%
where the time goes in v1:
time: 204 us
  Pallas kernels  197 us (97%)
  local copies, waits for them, and re-layouts  6.51 us (3%)
    pallas_call x1, Pallas kernels, on_device(): pl.pallas_call(functools.partial(kernel, n, n_fs, chunks, factor), out_sh...  197 us
    unnamed x5, local copies, waits for them, and re-layouts  6.51 us

profile of v1, /device:TPU:0, one launch (start us, length us, event | category | flops | bytes accessed | tf_op | source)
XLA Modules:
  0.0 203.9 jit_solution(2725283201755760793)
XLA Ops:
  0.6 196.8 %shard_map.76 = (bf16[128,2048]{1,0:T(8,128)(2,1)}, f32[512,1024]{1,0:T(8,128)}, f32[512,1024]{1,0:T(8,128)}) custom-call(bf16[128,2048]{1,0:T(8,128)(2,1)} %x_ref.1, bf16[128,2048]{1,0:T(8,128)(2,1)} %og_ref.1, bf16[1024,1024]{1,0:T(8,128)(2,1)} %pre_ref.1, bf16[512,1024]{1,0:T(8,128)(2,1)} %wu_ref.1, bf16[512,1024]{1,0:T(8,128)(2,1)} %wd_ref.1), custom_call_target="tpu_custom_call" | custom-call | tf_op jit(solution)/shard_map/pallas_call | solution.py:286
  197.4 1.9 copy.11
  199.3 0.0 copy-start
  199.3 3.3 %copy.12 = f32[512,1024]{1,0:T(8,128)} copy(f32[512,1024]{1,0:T(8,128)} %get-tuple-element.7) | data formatting | bytes 4194304
  202.6 0.0 copy-done
  202.6 1.3 copy.13
Async XLA Ops:
  199.3 3.3 %copy-start = (f32[512,1024]{1,0:T(8,128)S(1)}, f32[512,1024]{1,0:T(8,128)}, u32[]{:S(2)}) copy-start(f32[512,1024]{1,0:T(8,128)} %get-tuple-element.8) | copy-start | bytes 6291460

commit v2 on v1

--- a/solution.py
+++ b/solution.py
@@ -16,13 +16,24 @@
     x_ref, og_ref, pre_ref, wu_ref, wd_ref,
     gin_ref, gu_ref, gd_ref,
     x_all, og_all, wu_all, wd_all, sq, gp, rs, tbuf, prec, frec,
-    zs, zr, xs, xr, cs, cr, ts, tr, fsend, frecv,
+    pre, total, zs, zr, xs, xr, cs, cr, ts, tr, fsend, frecv, ls,
 ):
     r, f, t = lax.axis_index("rep"), lax.axis_index("fs"), lax.axis_index("tp")
     tok, d_model = og_ref.shape
     shard, cols = wd_ref.shape
     crow = shard // chunks
     partner = {"tp": 1 - t}
+    own_tokens = pl.ds(pl.multiple_of((f * 2 + t) * tok, tok), tok)
+    loads = [
+        pltpu.make_async_copy(src, dst, ls.at[i])
+        for i, (src, dst) in enumerate((
+            (pre_ref, pre),
+            (og_ref, og_all.at[own_tokens, :]),
+            (x_ref, x_all.at[own_tokens, :]),
+            (wd_ref, wd_all.at[r]),
+            (wu_ref, wu_all.at[r]),
+        ))
+    ]
     peers = [None] + [{"fs": lax.rem(f + d, n_fs)} for d in range(1, n_fs)]
     ahead = ({"rep": lax.rem(r + 1, n)}, {"rep": lax.rem(r + n - 1, n)})
     depth = (r, n - 1 - r)
@@ -58,9 +69,9 @@
     def piece(ref, j):
         return ref.at[pl.ds(pl.multiple_of(j * crow, crow), crow), :]
 
-    def send_own(phase, own, everyone):
+    def send_own(phase, own, everyone, when):
         for way in range(2):
-            @pl.when(has_next[way])
+            @pl.when(jnp.logical_and(has_next[way], when[way]))
             def _(way=way):
                 for j in range(chunks):
                     z_copy(
@@ -75,7 +86,6 @@
         remote(
             own, rows_of(everyone, f, t), cs.at[q, 0], cr.at[q, 0], partner
         ).start()
-        everyone[pl.ds(pl.multiple_of((f * 2 + t) * tok, tok), tok), :] = own[...]
 
     def spread_pass(q, everyone):
         for d in range(1, n_fs):
@@ -88,15 +98,18 @@
             there = rows_of(everyone, lax.rem(f + n_fs - d, n_fs), 1 - t)
             remote(there, there, cs.at[q, d], cr.at[q, d], partner).wait()
 
+    send_own(0, wd_ref, wd_all, (True, True))
     spread_start(0, og_ref, og_all)
-    send_own(0, wd_ref, wd_all)
-    wd_all[r] = wd_ref[...]
-    wu_all[r] = wu_ref[...]
+    send_own(1, wu_ref, wu_all, (depth[0] == 0, depth[1] == 0))
+    for load in loads:
+        load.start()
+    for load in loads:
+        load.wait()
     tile = 2 * tok
 
     def square(i, _):
         at = pl.ds(pl.multiple_of(i * tile, tile), tile)
-        linear = jnp.maximum(pre_ref[at, :].astype(F32), 0.0)
+        linear = jnp.maximum(pre[at, :].astype(F32), 0.0)
         sq[at, :] = (linear * linear).astype(BF16)
         return 0
 
@@ -149,43 +162,43 @@
 
         lax.fori_loop(0, chunks, one_piece, 0)
 
-    def last_round(phase, left, right, out):
+    def last_round(phase, left, right, out, low, high):
         def one_piece(j, _):
             at = pl.ds(pl.multiple_of(j * crow, crow), crow)
-            out[at, :] = partial(left, right, r, j)
+            total[...] = partial(left, right, r, j)
             for way in range(2):
                 @pl.when(has_prev[way])
                 def _(way=way):
                     block = piece(rs.at[phase, way, r], j)
                     z_copy(phase, way, n - 1, j, block, block).wait_recv()
-                    out[at, :] += rs[phase, way, r, at, :].astype(F32)
-            return 0
-
-        lax.fori_loop(0, chunks, one_piece, 0)
+                    total[...] += rs[phase, way, r, at, :].astype(F32)
+            out[at, :] = total[...].astype(BF16)
+            return 0
+
+        lax.fori_loop(low, high, one_piece, 0)
 
     def round_down(k, _):
         one_round(0, wd_all, og_all, sq, k)
+        send_own(1, wu_ref, wu_all, (depth[0] == k + 1, depth[1] == k + 1))
         return 0
 
     lax.fori_loop(0, n - 1, round_down, 0)
-    send_own(1, wu_ref, wu_all)
     spread_pass(1, x_all)
 
     def make_grad_pre(i, _):
         at = pl.ds(pl.multiple_of(i * tile, tile), tile)
-        total = jnp.zeros((tile, cols), F32)
+        acc = jnp.zeros((tile, cols), F32)
         for s in range(n):
-            total += jnp.dot(
+            acc += jnp.dot(
                 og_all[at, s * shard:(s + 1) * shard], wd_all[s],
                 preferred_element_type=F32,
             )
-        linear = jnp.maximum(pre_ref[at, :].astype(F32), 0.0)
-        gp[at, :] = (total * 2.0 * linear).astype(BF16)
+        linear = jnp.maximum(pre[at, :].astype(F32), 0.0)
+        gp[at, :] = (acc * 2.0 * linear).astype(BF16)
         return 0
 
     lax.fori_loop(0, n_fs, make_grad_pre, 0)
     spread_end(1, x_all)
-    last_round(0, og_all, sq, gd_ref)
 
     def cross(s):
         return remote(tbuf.at[s, 1 - t], prec.at[s], ts.at[s], tr.at[s], partner)
@@ -235,32 +248,30 @@
 
         lax.fori_loop(0, 2, body, 0)
 
+    one_round(1, wu_all, x_all, gp, 0)
     block_term(r)
+    for_new(0, block_term)
+    last_round(0, og_all, sq, gd_ref, 0, chunks)
+    chip_sum(r)
 
     def round_up(k, _):
         one_round(1, wu_all, x_all, gp, k)
         for_new(k, block_term)
-
-        @pl.when(k == 0)
-        def _():
-            chip_sum(r)
-
-        @pl.when(k > 0)
-        def _():
-            for_new(k - 1, chip_sum)
+        for_new(k - 1, chip_sum)
         return 0
 
-    lax.fori_loop(0, n - 1, round_up, 0)
+    lax.fori_loop(1, n - 1, round_up, 0)
     for_new(n - 2, chip_sum)
-    last_round(1, x_all, gp, gu_ref)
+    last_round(1, x_all, gp, gu_ref, 0, chunks - 1)
 
     own_rows = pl.ds(pl.multiple_of(f * tok, tok), tok)
     for s in range(n):
-        total = prec[s, own_rows, :].astype(F32)
+        acc = prec[s, own_rows, :].astype(F32)
         for d in range(1, n_fs):
             out_copy(s, d).wait()
-            total += frec[s, d - 1].astype(F32)
-        gin_ref[:, s * shard:(s + 1) * shard] = total.astype(BF16)
+            acc += frec[s, d - 1].astype(F32)
+        gin_ref[:, s * shard:(s + 1) * shard] = acc.astype(BF16)
+    last_round(1, x_all, gp, gu_ref, chunks - 1, chunks)
 
     for way in range(2):
         @pl.when(has_next[way])
@@ -287,10 +298,10 @@
         functools.partial(kernel, n, n_fs, chunks, factor),
         out_shape=(
             jax.ShapeDtypeStruct((tok, d_model), BF16),
-            jax.ShapeDtypeStruct((shard, cols), F32),
-            jax.ShapeDtypeStruct((shard, cols), F32),
+            jax.ShapeDtypeStruct((shard, cols), BF16),
+            jax.ShapeDtypeStruct((shard, cols), BF16),
         ),
-        in_specs=[vmem] * 5,
+        in_specs=[pl.BlockSpec(memory_space=pl.ANY)] * 5,
         out_specs=(vmem,) * 3,
         scratch_shapes=[
             pltpu.VMEM((group, d_model), BF16),
@@ -303,6 +314,8 @@
             pltpu.VMEM((n, 2, n_fs * tok, shard), BF16),
             pltpu.VMEM((n, n_fs * tok, shard), BF16),
             pltpu.VMEM((n, n_fs - 1, tok, shard), BF16),
+            pltpu.VMEM((group, cols), BF16),
+            pltpu.VMEM((shard // chunks, cols), F32),
             dma((2, 2, n, chunks)),
             dma((2, 2, n, chunks)),
             dma((2, n_fs)),
@@ -313,12 +326,13 @@
             dma((n,)),
             dma((n, n_fs)),
             dma((n, n_fs)),
+            dma((5,)),
         ],
         compiler_params=pltpu.CompilerParams(
             collective_id=0, has_side_effects=True, vmem_limit_bytes=67043328
         ),
     )(inputs, out_grad, pre_act, w_up, w_down_t)
-    return grad_in, grad_up, grad_down_t
+    return grad_in, grad_up.astype(F32), grad_down_t.astype(F32)
 
 
 def solution(mesh):

time: 204 us -> 201 us (0.985)
  local copies, waits for them, and re-layouts: 6.51 us -> 0.8 us
  other arithmetic: 0 us -> 4.44 us
    unnamed x5, local copies, waits for them, and re-layouts: 6.51 us -> 0.8 us
    convert_element_type x0 -> x2, other arithmetic: none -> 4.44 us  [on_device(): return (grad_in, grad_up.astype(F32), grad_down_t.astype(F32))]
where the time goes in v2:
time: 201 us
  Pallas kernels  195 us (97%)
  other arithmetic  4.44 us (2%)
    pallas_call x1, Pallas kernels, on_device(): pl.pallas_call(functools.partial(kernel, n, n_fs, chunks, factor), out_sh...  195 us
    convert_element_type x2, other arithmetic, on_device(): return (grad_in, grad_up.astype(F32), grad_down_t.astype(F32))  4.44 us

profile of v2, /device:TPU:0, one launch (start us, length us, event | category | flops | bytes accessed | tf_op | source)
XLA Modules:
  0.0 201.3 jit_solution(9214245214395969893)
XLA Ops:
  0.6 195.4 %shard_map.76 = (bf16[128,2048]{1,0:T(8,128)(2,1)}, bf16[512,1024]{1,0:T(8,128)(2,1)}, bf16[512,1024]{1,0:T(8,128)(2,1)}) custom-call(bf16[128,2048]{1,0:T(8,128)(2,1)} %x_ref.1, bf16[128,2048]{1,0:T(8,128)(2,1)} %og_ref.1, bf16[1024,1024]{1,0:T(8,128)(2,1)} %pre_ref.1, bf16[512,1024]{1,0:T(8,128)(2,1)} %wu_ref.1, bf16[512,1024]{1,0:T(8,128)(2,1)} %wd_ref.1), custom_call_target="tpu_custom_call" | custom-call | tf_op jit(solution)/shard_map/pallas_call | solution.py:297
  196.0 0.0 copy-start
  196.0 2.9 %convert_element_type.6 = f32[512,1024]{1,0:T(8,128)} convert(bf16[512,1024]{1,0:T(8,128)(2,1)} %get-tuple-element.7) | non-fusion elementwise | flops 524288 | bytes 3145728 | tf_op jit(solution)/shard_map/convert_element_type | solution.py:335
  198.9 0.0 copy-done
  198.9 0.0 copy-start.1
  198.9 1.6 convert_element_type.7
  200.5 0.0 copy-done.1
  200.5 0.8 copy.9
Async XLA Ops:
  196.0 2.9 %copy-start = (bf16[512,1024]{1,0:T(8,128)(2,1)S(1)}, bf16[512,1024]{1,0:T(8,128)(2,1)}, u32[]{:S(2)}) copy-start(bf16[512,1024]{1,0:T(8,128)(2,1)} %get-tuple-element.8) | copy-start | bytes 3145732
  198.9 1.6 copy-start.1
